TPU v7x, 512 devices: a whole 4x4x16 slice. The times are simulated.
512 devices in a mesh: sp: 16 (over z), fs: 4 (over y), tp: 8 (over x, core).
Axes of the slice: x: 4, y: 4, z: 16, core: 2. Of those that a mesh axis runs over, the one named last changes fastest.
Arguments:
- tokens: bfloat16 [16384, 2048], P(('fs', 'sp', 'tp')), parts along dimension 0, may hold values from -6 to 6
- norm_gain: bfloat16 [2048], replicated, may hold values from 0.099609375 to 1.8984375
- w_pool_in: bfloat16 [2048, 1024], P('sp', 'tp'), may hold values from -0.125 to 0.125
- w_query: bfloat16 [2048, 1024], P('sp', 'tp'), may hold values from -0.125 to 0.125
- w_key: bfloat16 [2048, 1024], P('sp', 'tp'), may hold values from -0.125 to 0.125
- w_value: bfloat16 [2048, 1024], P('sp', 'tp'), may hold values from -0.125 to 0.125
- w_gate: bfloat16 [2048, 1024], P('sp', 'tp'), may hold values from -0.125 to 0.125
- w_beta: bfloat16 [2048, 8], replicated, may hold values from -0.125 to 0.125
- w_decay: bfloat16 [2048, 8], replicated, may hold values from -0.5 to 0.5
- conv_weight: float32 [3, 4, 1024], P(None, None, 'tp'), may hold values from -3 to 3
- a_log: float32 [8], P('tp'), may hold values from -20 to -1.7, as said below
- decay_extra: float32 [16384, 8], P(('fs', 'sp'), 'tp'), parts along dimension 0, may hold values from -1.4 to 0
- w_mix: bfloat16 [8, 128, 128], P('tp'), may hold values from -0.5 to 0.5
- pool_scale: float32 [1024], P('tp'), may hold values from 0.1 to 1.9
- delta_gain: float32 [128], replicated, may hold values from 0.1 to 1.9
- w_out_pool: bfloat16 [1024, 2048], P('tp', 'sp'), may hold values from -0.125 to 0.125
- w_out_delta: bfloat16 [1024, 2048], P('tp', 'sp'), may hold values from -0.125 to 0.125
Outputs:
- mixed: bfloat16 [16384, 2048], P(('fs', 'sp', 'tp')), parts along dimension 0
There are 4 independent parts, one for each index of `fs`. A program takes and returns all parts, laid end to end along the dimension named above; an argument that names none is the same for every part. Nothing has to cross between parts.
Inputs may be any that keep to these rules, and one draw needn't show every extreme that they name: `a_log`: logarithm of each head's base decay rate.
All inputs are finite; a program needn't handle non-finite values.
Results may differ from a plain program's by a relative error of at most 0.018.
Values may be sent and summed in bfloat16 or wider, within the bound.
No kernel may reach another device: no remote copies, remote signals or barrier semaphores. Data moves between devices by JAX's collectives and lax.ppermute only.
A program may use at most 64 MiB of HBM per device.

v0:
```python
import jax
import jax.numpy as jnp
from jax import lax
from jax.sharding import PartitionSpec as P

BLOCK = 64
eps = 1e-06
windows = (2, 4, 8, 16)
tail_rows = 15


def turned_gather(arrays, axis, dims):
    turned = [jnp.moveaxis(a, dim, 0) for a, dim in zip(arrays, dims)]
    both = jnp.concatenate([t.reshape(len(t), -1) for t in turned], axis=1)
    out, at, finished = (lax.all_gather(both, axis, axis=0, tiled=True), 0, [])
    for t, dim in zip(turned, dims):
        slab = out[:, at : at + t[0].size].reshape(-1, *t.shape[1:])
        finished.append(jnp.moveaxis(slab, 0, dim))
        at += t[0].size
    return tuple(finished)


def copy_for_each(x, axis):
    copies = jnp.broadcast_to(x, (lax.axis_size(axis), *x.shape))
    return lax.all_to_all(copies, axis, split_axis=0, concat_axis=0, tiled=True)


def laid_out(blocks, dim):
    lengths = list(blocks.shape[1:])
    lengths[dim] *= blocks.shape[0]
    return jnp.moveaxis(blocks, 0, dim).reshape(lengths)


def gather_directly(x, axis, dim):
    blocks = copy_for_each(x, axis)
    return laid_out(blocks, dim)


def from_behind(block, axis, distance):
    devices = range(lax.axis_size(axis))
    route = [(i - distance, i) for i in devices if i - distance in devices]
    return lax.ppermute(block, axis, route)


def entering(x, axis, join, neutral):
    place = lax.axis_index(axis)
    gathered = jax.tree.map(
        lambda a, kind: lax.all_gather(a.astype(kind), axis), x, (jnp.bfloat16, jnp.bfloat16)
    )
    state = jax.tree.map(lambda a, e: jnp.zeros_like(a) + jnp.asarray(e, a.dtype), x, neutral)

    def one(hop, state):
        return join(
            state,
            jax.tree.map(
                lambda a, own: lax.dynamic_index_in_dim(a, hop, 0, False).astype(own.dtype),
                gathered,
                x,
            ),
        )

    return lax.fori_loop(0, place, one, state)


def side_by_side(arrays, axis, dim, along):
    ends, at = ([], 0)
    for a in arrays[:-1]:
        at += a.shape[along]
        ends.append(at)
    both = jnp.concatenate(arrays, axis=along)
    return tuple(jnp.split(lax.all_gather(both, axis, axis=dim, tiled=True), ends, axis=along))


def rms_rows(values, gain):
    floats = values.astype(jnp.float32)
    scale = lax.rsqrt(jnp.mean(floats * floats, axis=-1, keepdims=True) + eps)
    return (floats * scale * gain.astype(jnp.float32)).astype(jnp.bfloat16)


def unit_rows(values):
    return values * lax.rsqrt(jnp.sum(values * values, axis=-1, keepdims=True) + eps)


def block_terms(query, keys, values, log_gate, strength, block):
    heads, length, width = keys.shape
    count = length // block

    def split(tensor):
        return tensor.reshape(heads, count, block, tensor.shape[-1])

    query_part, key_part, value_part = (split(query), split(keys), split(values))
    gate_cum = jnp.cumsum(log_gate.reshape(heads, count, block), axis=-1)
    beta_part = strength.reshape(heads, count, block)[..., None]
    lower_mask = jnp.tril(jnp.ones((block, block), dtype=bool))
    strict_mask = jnp.tril(jnp.ones((block, block), dtype=bool), k=-1)
    gaps = gate_cum[..., :, None] - gate_cum[..., None, :]
    decay_tab = jnp.where(lower_mask, jnp.exp(jnp.where(lower_mask, gaps, 0.0)), 0.0)
    key_scaled_beta = key_part * beta_part
    value_beta = value_part * beta_part
    corr_lower = jnp.where(
        strict_mask, jnp.einsum("hnid,hnjd->hnij", key_scaled_beta, key_part) * decay_tab, 0.0
    )
    identity = jnp.eye(block, dtype=jnp.float32)
    inverse = lax.linalg.triangular_solve(
        identity + corr_lower,
        jnp.broadcast_to(identity, corr_lower.shape),
        left_side=True,
        lower=True,
    )
    fixed_values = jnp.einsum("hnij,hnjd->hnid", inverse, value_beta)
    key_weights = jnp.einsum(
        "hnij,hnjd->hnid", inverse, key_scaled_beta * jnp.exp(gate_cum)[..., None]
    )
    scores = jnp.where(
        lower_mask, jnp.einsum("hnid,hnjd->hnij", query_part, key_part) * decay_tab, 0.0
    )
    key_decayed = key_part * jnp.exp(gate_cum[..., -1:] - gate_cum)[..., None]
    query_gated = query_part * jnp.exp(gate_cum)[..., None]
    terms = (query_gated, key_decayed, fixed_values, key_weights, scores, gate_cum[..., -1])
    return tuple((jnp.moveaxis(tensor, 1, 0) for tensor in terms))


def carry_step(state, inputs):
    query_gated, key_decayed, fixed_values, key_weights, scores, last_gate = inputs
    fresh = fixed_values - jnp.einsum("hcd,hde->hce", key_weights, state)
    output = jnp.einsum("hcd,hde->hce", query_gated, state) + jnp.einsum(
        "hij,hje->hie", scores, fresh
    )
    state = state * jnp.exp(last_gate)[:, None, None] + jnp.einsum(
        "hcd,hce->hde", key_decayed, fresh
    )
    return (state, output)


def compose_step(carry, inputs):
    linear, offset = carry
    query_gated, key_decayed, fixed_values, key_weights, scores, last_gate = inputs
    fade = jnp.exp(last_gate)[:, None, None]
    moved = jnp.einsum("hcd,hde->hce", key_weights, linear)
    linear = fade * linear - jnp.einsum("hcd,hce->hde", key_decayed, moved)
    fresh = fixed_values - jnp.einsum("hcd,hde->hce", key_weights, offset)
    offset = fade * offset + jnp.einsum("hcd,hce->hde", key_decayed, fresh)
    return ((linear, offset), None)


def apply_map(linear, state):
    return jnp.einsum("hij,hjk->hik", linear, state)


def combine_maps(earlier, later):
    return (apply_map(later[0], earlier[0]), apply_map(later[0], earlier[1]) + later[1])


def per_device(
    tokens,
    norm_gain,
    w_pool_in,
    w_query,
    w_key,
    w_value,
    w_gate,
    w_beta,
    w_decay,
    conv_weight,
    a_log,
    decay_extra,
    w_mix,
    pool_scale,
    delta_gain,
    w_out_pool,
    w_out_delta,
):
    pool_w, query_w, key_w, value_w, gate_w, outp_w, outd_w = turned_gather(
        (w_pool_in, w_query, w_key, w_value, w_gate, w_out_pool, w_out_delta),
        "sp",
        (0, 0, 0, 0, 0, 1, 1),
    )
    rows_all = gather_directly(tokens, "tp", 0)
    norm_result = rms_rows(rows_all, norm_gain)
    length = norm_result.shape[0]

    def project(weight):
        return jnp.dot(norm_result, weight, preferred_element_type=jnp.float32).astype(jnp.bfloat16)

    pool_in = project(pool_w)
    query_raw = project(query_w)
    key_raw = project(key_w)
    value_raw = project(value_w)
    gate_raw = project(gate_w)
    heads_dev = a_log.shape[0]
    head_dim = query_raw.shape[1] // heads_dev
    width_dev = heads_dev * head_dim
    all_heads = w_beta.shape[1]
    lane = lax.axis_index("tp")
    both_pre = jnp.dot(
        norm_result, jnp.concatenate([w_beta, w_decay], axis=1), preferred_element_type=jnp.float32
    )
    beta_pre = lax.dynamic_slice_in_dim(both_pre[:, :all_heads], lane * heads_dev, heads_dev, 1)
    forget_logits = lax.dynamic_slice_in_dim(
        both_pre[:, all_heads:], lane * heads_dev, heads_dev, 1
    )
    raw_three = jnp.concatenate([query_raw, key_raw, value_raw], axis=1)
    tails = jnp.concatenate(
        [pool_in[length - tail_rows :], raw_three[length - tail_rows :]], axis=1
    )
    prior_state = from_behind(tails, "sp", 1)
    pool_width_dev = pool_in.shape[1]
    source_rows = pool_in.astype(jnp.float32)
    extended = jnp.concatenate(
        [prior_state[:, :pool_width_dev].astype(jnp.float32), source_rows], axis=0
    )
    running = jnp.concatenate(
        [jnp.zeros((1, pool_width_dev), jnp.float32), jnp.cumsum(extended, axis=0)], axis=0
    )
    groups_dev = w_mix.shape[0]
    group_dim = w_mix.shape[1]
    group = lane * groups_dev + jnp.arange(pool_width_dev) // group_dim
    span = (2 ** (1 + group % 4)).astype(jnp.int32)
    ending = running[tail_rows + 1 : tail_rows + 1 + length]
    window_sum = jnp.zeros((length, pool_width_dev), jnp.float32)
    for width in windows:
        lagged = running[tail_rows + 1 - width : tail_rows + 1 - width + length]
        window_sum = window_sum + jnp.where(span[None, :] == width, ending - lagged, 0.0)
    positions = lax.axis_index("sp") * length + jnp.arange(length)
    counts = jnp.minimum(positions[:, None] + 1, span[None, :]).astype(jnp.float32)
    pooled = (window_sum / counts - source_rows).astype(jnp.bfloat16)
    mixed_pool = jnp.einsum(
        "sgc,gcd->sgd",
        pooled.reshape(length, groups_dev, group_dim),
        w_mix,
        preferred_element_type=jnp.float32,
    )
    pool_out = (mixed_pool.reshape(length, pool_width_dev) * pool_scale).astype(jnp.bfloat16)
    taps = conv_weight.shape[1]
    kernel = jnp.transpose(conv_weight, (1, 0, 2)).reshape(taps, 3 * width_dev)
    stacked = jnp.concatenate(
        [prior_state[tail_rows - (taps - 1) :, pool_width_dev:], raw_three], axis=0
    ).astype(jnp.float32)
    conv = jnp.zeros((length, 3 * width_dev), jnp.float32)
    for tap in range(taps):
        conv = conv + stacked[tap : tap + length] * kernel[tap]
    after_silu = jax.nn.silu(conv)

    def heads_first(tensor):
        return jnp.transpose(tensor.reshape(length, heads_dev, head_dim), (1, 0, 2))

    query = unit_rows(heads_first(after_silu[:, :width_dev])) * head_dim ** (-0.5)
    keys = unit_rows(heads_first(after_silu[:, width_dev : 2 * width_dev]))
    values = heads_first(after_silu[:, 2 * width_dev :])
    strength = jax.nn.sigmoid(beta_pre).T
    log_gate = (-jnp.exp(a_log)[None, :] * jax.nn.softplus(forget_logits) + decay_extra).T
    terms = block_terms(query, keys, values, log_gate, strength, BLOCK)
    identity = jnp.broadcast_to(
        jnp.eye(head_dim, dtype=jnp.float32), (heads_dev, head_dim, head_dim)
    )
    empty = jnp.zeros((heads_dev, head_dim, head_dim), jnp.float32)
    (linear, offset), _ = lax.scan(compose_step, (identity, empty), terms)
    prefix = entering((linear, offset), "sp", combine_maps, (identity, empty))
    incoming = prefix[1]
    _, outputs = lax.scan(carry_step, incoming, terms)
    attended = jnp.transpose(outputs, (1, 0, 2, 3)).reshape(heads_dev, length, head_dim)
    normal_out = (
        attended
        * lax.rsqrt(jnp.mean(attended * attended, axis=-1, keepdims=True) + eps)
        * delta_gain
    )
    gated = normal_out * jax.nn.silu(heads_first(gate_raw.astype(jnp.float32)))
    delta_out = jnp.transpose(gated, (1, 0, 2)).reshape(length, width_dev).astype(jnp.bfloat16)
    groups = lax.axis_size("tp")
    rows = length // groups
    both = jnp.concatenate([pool_out, delta_out], axis=1)
    arrived = lax.all_to_all(both, "tp", split_axis=0, concat_axis=0, tiled=True).reshape(
        groups, rows, pool_width_dev + width_dev
    )
    pool_rows, delta_rows = side_by_side((outp_w, outd_w), "tp", 0, 1)
    part_pool = jnp.einsum(
        "jrp,jpd->jrd",
        arrived[..., :pool_width_dev],
        pool_rows.reshape(groups, pool_width_dev, -1),
        preferred_element_type=jnp.float32,
    )
    part_delta = jnp.einsum(
        "jrp,jpd->jrd",
        arrived[..., pool_width_dev:],
        delta_rows.reshape(groups, width_dev, -1),
        preferred_element_type=jnp.float32,
    )
    value_partial_rows = lax.optimization_barrier(
        (part_pool + part_delta).astype(jnp.bfloat16)
    ).astype(jnp.float32)
    result = jnp.sum(value_partial_rows, axis=0)
    return result.astype(jnp.bfloat16)


def solution(mesh):
    placed = (
        P(("fs", "sp", "tp"), None),
        P(),
        P("sp", "tp"),
        P("sp", "tp"),
        P("sp", "tp"),
        P("sp", "tp"),
        P("sp", "tp"),
        P(),
        P(),
        P(None, None, "tp"),
        P("tp"),
        P(("fs", "sp"), "tp"),
        P("tp", None, None),
        P("tp"),
        P(),
        P("tp", "sp"),
        P("tp", "sp"),
    )
    return jax.shard_map(
        per_device,
        mesh=mesh,
        in_specs=placed,
        out_specs=P(("fs", "sp", "tp"), None),
        check_vma=False,
    )
```

profile of v0, /device:TPU:1, one launch (start us, length us, event | category | flops | bytes accessed | tf_op | source)
XLA Modules:
  0.0 249.7 jit_solution(6866411914422944330)
XLA Ops:
  6.5 0.9 copy.78
  7.4 0.9 copy.79
  8.3 0.9 copy.80
  9.2 0.9 copy.81
  10.1 0.9 copy.82
  11.0 0.8 bitcast_dynamic-update-slice_fusion.1
  11.8 0.8 bitcast_dynamic-update-slice_fusion
  12.5 0.7 copy-done.2
  13.3 2.0 broadcast_in_dim.91
  15.3 10.4 %all-to-all-start = ((bf16[8,32,2048]{2,1,0:T(8,128)(2,1)}), bf16[8,32,2048]{2,1,0:T(8,128)(2,1)S(1)}, u32[]{:S(2)}, u32[]{:S(2)}) async-start(bf16[8,32,2048]{2,1,0:T(8,128)(2,1)} %broadcast_in_dim.91), calls=%async_computation | async-start | bytes 2097152 | tf_op jit(solution)/shard_map/all_to_all | solution.py:25
  26.5 71.0 %all-gather.5.cloned.1.call-done = bf16[2048,896]{0,1:T(8,128)(2,1)} async-done(((bf16[128,896]{0,1:T(8,128)(2,1)}), bf16[2048,896]{0,1:T(8,128)(2,1)}) %all-gather.5.cloned.1.call-update) | async-done | bytes 3670032 | tf_op jit(solution)/shard_map/all_gather | solution.py:15
  97.5 1.3 slice_bitcast_fusion.1
  98.8 1.1 pad_maximum_fusion
  100.1 0.3 multiply_reduce_fusion
  100.5 0.3 fusion.59
  100.8 0.4 fusion.100
  101.4 0.2 reduce_window_sum.30
  101.6 0.2 slice_reduce_fusion
  101.8 1.5 fusion.131
  103.3 1.5 convolution_convert_fusion.1
  104.8 1.5 convolution_convert_fusion.2
  106.3 1.5 convolution_convert_fusion.3
  107.8 3.3 %collective-permute-start = (bf16[15,512]{1,0:T(8,128)(2,1)S(1)}, bf16[15,512]{1,0:T(8,128)(2,1)S(1)}, u32[]{:S(2)}, u32[]{:S(2)}) collective-permute-start(bf16[15,512]{1,0:T(8,128)(2,1)S(1)} %fusion.115), channel_id=1, source_target_pairs={{0,32},{32,64},{64,96},{96,128},{128,160},{160,192},{192,224},{224... | collective-permute-start | bytes 46088 | tf_op jit(solution)/shard_map/ppermute | solution.py:42
  111.2 0.7 collective-permute-done
  112.3 0.2 divide_multiply_fusion
  112.9 0.2 fusion.65
  113.1 19.7 %custom-call.3 = f32[1,4,1,64,64]{3,4,2,1,0:T(8,128)S(1)} custom-call(f32[1,4,1,64,64]{4,3,2,1,0:T(8,128)S(1)} %fusion.65), custom_call_target="InvertDiagBlocksLowerTriangular" | custom-call | tf_op jit(solution)/shard_map/triangular_solve | solution.py:104
  132.8 0.4 fusion.91
  133.2 0.2 convolution_bitcast_fusion.3
  133.4 0.3 convolution_bitcast_fusion.4
  133.8 9.7 %while.39 = (s32[]{:T(128)}, f32[1,128,128]{2,1,0:T(8,128)S(1)}, f32[1,128,128]{2,1,0:T(8,128)S(1)}, f32[4,1]{0,1:T(1,128)S(1)}, bf16[4,1,64,128]{3,2,1,0:T(8,12...) while((s32[]{:T(128)}, f32[1,128,128]{2,1,0:T(8,128)S(1)}, ...), condition=%wide.region_6.7_spmd.clone, body=%wide.region_5.6_spmd.clone.sunk | while | flops 8503299 | bytes 757378 | solution.py:257
  133.8 0.6 fusion.206
  134.5 0.9 fusion.208
  135.4 0.9 fusion.207
  136.3 0.6 fusion.206
  136.9 0.9 fusion.208
  137.8 0.9 fusion.207
  138.7 0.6 fusion.206
  139.3 0.9 fusion.208
  140.2 0.9 fusion.207
  141.1 0.6 fusion.206
  141.7 0.9 fusion.208
  142.6 0.9 fusion.207
  143.5 0.2 fusion.61
  143.8 26.1 %all-gather = bf16[16,128,128]{2,1,0:T(8,128)(2,1)S(1)} all-gather(bf16[1,128,128]{2,1,0:T(8,128)(2,1)S(1)} %convert_element_type.116), channel_id=2, replica_groups=mesh['sp'=16,'fs'=4,'tp'=8] {'sp'}, dimensions={0}, use_global_device_ids=true | all-gather | bytes 557056 | tf_op jit(solution)/shard_map/all_gather | solution.py:48
  169.9 24.1 %all-gather.1 = bf16[16,128,128]{2,1,0:T(8,128)(2,1)S(1)} all-gather(bf16[1,128,128]{2,1,0:T(8,128)(2,1)S(1)} %convert_element_type.117), channel_id=3, replica_groups=mesh['sp'=16,'fs'=4,'tp'=8] {'sp'}, dimensions={0}, use_global_device_ids=true | all-gather | bytes 557056 | tf_op jit(solution)/shard_map/all_gather | solution.py:48
  194.0 7.4 %while.38 = (s32[]{:T(128)}, f32[1,128,128]{2,1,0:T(8,128)S(1)}, f32[4,1,64,128]{3,2,1,0:T(8,128)S(1)}, f32[4,1]{0,1:T(1,128)S(1)}, bf16[4,1,64,128]{3,2,1,0:T(8...) while((s32[]{:T(128)}, f32[1,128,128]{2,1,0:T(8,128)S(1)}, ...), condition=%wide.region_11.12_spmd, body=%wide.region_10.11_spmd.sunk | while | flops 7397378 | bytes 510085 | solution.py:260
  194.0 0.6 fusion.195
  194.9 0.8 fusion.196
  195.9 0.6 fusion.195
  196.8 0.8 fusion.196
  197.7 0.6 fusion.195
  198.6 0.8 fusion.196
  199.6 0.6 fusion.195
  200.4 0.8 fusion.196
  201.6 0.3 fusion.110
  201.9 1.5 fusion.90
  203.4 0.7 pad_maximum_fusion.1
  204.1 27.8 %all-to-all-start.1 = ((bf16[8,32,256]{2,1,0:T(8,128)(2,1)}), bf16[8,32,256]{2,1,0:T(8,128)(2,1)S(1)}, u32[]{:S(2)}, u32[]{:S(2)}) async-start(bf16[8,32,256]{2,1,0:T(8,128)(2,1)} %pad_maximum_fusion.1), calls=%async_computation.1 | async-start | bytes 262144 | tf_op jit(solution)/shard_map/all_to_all | solution.py:272
  231.9 6.0 %fusion.129 = (bf16[1024,2048]{1,0:T(8,128)(2,1)}, bf16[1024,2048]{1,0:T(8,128)(2,1)}) fusion(bf16[1024,4096]{1,0:T(8,128)(2,1)} %all-gather.7.cloned.1.call-done), kind=kLoop, calls=%fused_computation.205 | loop fusion | bytes 16777216 | tf_op jit(solution)/shard_map/split | solution.py:71
  237.9 3.0 %fusion.98 = f32[8,32,2048]{2,1,0:T(8,128)S(1)} fusion(bf16[8,128,2048]{2,1,0:T(8,128)(2,1)} %bitcast.262, bf16[8,32,256]{2,1,0:T(8,128)(2,1)S(1)} %all-to-all-done.1), kind=kOutput, calls=%fused_computation.129 | convolution fusion | flops 134217728 | bytes 6356992 | tf_op jit(solution)/shard_map/jrp,jpd->jrd/dot_general | solution.py:276
  240.9 0.4 copy-done.1
  241.4 0.7 fusion.57
  242.1 0.8 reduce_sum.52
  (95 shorter events, 3.4 us)
Async XLA Ops:
  6.5 195.1 %copy-start = (bf16[1,128,128]{2,1,0:T(8,128)(2,1)S(1)}, bf16[1,128,128]{2,1,0:T(8,128)(2,1)}, u32[]{:S(2)}) copy-start(bf16[1,128,128]{2,1,0:T(8,128)(2,1)} %param.35) | copy-start | bytes 98308
  6.5 19.9 %copy-start.6 = (bf16[2048]{0:T(1024)(128)(2,1)S(1)}, bf16[2048]{0:T(1024)(128)(2,1)}, u32[]{:S(2)}) copy-start(bf16[2048]{0:T(1024)(128)(2,1)} %param.24) | copy-start | bytes 12292
  6.5 90.9 %all-gather.5.cloned.1.call-start = ((), (), s32[]{:S(2)}) async-start(), calls=%async_computation.2 | async-start | bytes 3899392 | tf_op jit(solution)/shard_map/all_gather | solution.py:15
  12.5 0.7 copy-start.2
  15.3 84.7 %copy-start.5 = (f32[3,4,128]{2,1,0:T(4,128)S(1)}, f32[3,4,128]{2,1,0:T(4,128)}, u32[]{:S(2)}) copy-start(f32[3,4,128]{2,1,0:T(4,128)} %param.32) | copy-start | bytes 18436
  15.3 84.9 %all-to-all-start = ((bf16[8,32,2048]{2,1,0:T(8,128)(2,1)}), bf16[8,32,2048]{2,1,0:T(8,128)(2,1)S(1)}, u32[]{:S(2)}, u32[]{:S(2)}) async-start(bf16[8,32,2048]{2,1,0:T(8,128)(2,1)} %broadcast_in_dim.91), calls=%async_computation | async-start | bytes 2097152 | tf_op jit(solution)/shard_map/all_to_all | solution.py:25
  25.7 206.2 %all-gather.7.cloned.1.call-start = ((), (), s32[]{:S(2)}) async-start(), calls=%async_computation.3 | async-start | bytes 9437184 | tf_op jit(solution)/shard_map/all_gather | solution.py:71
  98.8 2.1 copy-start.3
  98.8 2.1 copy-start.4
  98.8 2.4 copy-start.7
  107.8 4.2 %collective-permute-start = (bf16[15,512]{1,0:T(8,128)(2,1)S(1)}, bf16[15,512]{1,0:T(8,128)(2,1)S(1)}, u32[]{:S(2)}, u32[]{:S(2)}) collective-permute-start(bf16[15,512]{1,0:T(8,128)(2,1)S(1)} %fusion.115), channel_id=1, source_target_pairs={{0,32},{32,64},{64,96},{96,128},{128,160},{160,192},{192,224},{224... | collective-permute-start | bytes 46088 | tf_op jit(solution)/shard_map/ppermute | solution.py:42
  169.9 31.9 %copy-start.8 = (f32[128]{0:T(128)S(1)}, f32[128]{0:T(128)}, u32[]{:S(2)}) copy-start(f32[128]{0:T(128)} %param.36) | copy-start | bytes 1540
  169.9 32.0 %copy-start.9 = (f32[128]{0:T(128)S(1)}, f32[128]{0:T(128)}, u32[]{:S(2)}) copy-start(f32[128]{0:T(128)} %param.37) | copy-start | bytes 1540
  204.1 33.9 %all-to-all-start.1 = ((bf16[8,32,256]{2,1,0:T(8,128)(2,1)}), bf16[8,32,256]{2,1,0:T(8,128)(2,1)S(1)}, u32[]{:S(2)}, u32[]{:S(2)}) async-start(bf16[8,32,256]{2,1,0:T(8,128)(2,1)} %pad_maximum_fusion.1), calls=%async_computation.1 | async-start | bytes 262144 | tf_op jit(solution)/shard_map/all_to_all | solution.py:272
  237.9 3.5 %copy-start.1 = (bf16[1024,2048]{1,0:T(8,128)(2,1)S(1)}, bf16[1024,2048]{1,0:T(8,128)(2,1)}, u32[]{:S(2)}) copy-start(bf16[1024,2048]{1,0:T(8,128)(2,1)} %get-tuple-element.294) | copy-start | bytes 12582916
Sparse Core Ops, SparseCore 0:
  13.4 84.0 all-gather.4
  100.0 65.0 all-gather.6
where the time goes:
time: 251 us; the launch traced here: 250 us
  waiting for transfers between devices  71.7 us (29%)
  blocking collectives  50.2 us (20%)
  starting transfers between devices  41.6 us (17%)
  matrix products  24.9 us (10%)
  other arithmetic  24.6 us (10%)
  local copies, waits for them, and re-layouts  22.1 us (9%)
  between operations  14.5 us (6%)
    all_gather x1, waiting for transfers between devices, turned_gather(): out, at, finished = (lax.all_gather(both, axis, axis=0, tiled=True), 0, [])  71 us
    all_gather x2, blocking collectives, entering(): lax.all_gather(a.astype(kind), axis)  50.2 us
    all_to_all x1, starting transfers between devices, per_device(): lax.all_to_all(both, 'tp', split_axis=0, concat_axis=0, tiled=True)  27.8 us
    another operation x1, other arithmetic, block_terms(): lax.linalg.triangular_solve(identity + corr_lower, jnp.broadcast_to(ident...  19.7 us
    all_to_all x1, starting transfers between devices, copy_for_each(): return lax.all_to_all(copies, axis, split_axis=0, concat_axis=0, tiled=True)  10.4 us
    dot_general x5, matrix products, project(): jnp.dot(norm_result, weight, preferred_element_type=jnp.float32)  7.41 us
    unnamed x31, local copies, waits for them, and re-layouts  6.34 us
    split x1, local copies, waits for them, and re-layouts, side_by_side(): jnp.split(lax.all_gather(both, axis, axis=dim, tiled=True), ends, axis=al...  6.02 us
  transfers between devices with their start and end apart: 5, of which 2 were waited for; matrix products, arithmetic and copies ran while one was open for 24% of the time, Pallas kernels for 0%

commit v1 on v0

--- a/solution.py
+++ b/solution.py
@@ -12,7 +12,13 @@
 def turned_gather(arrays, axis, dims):
     turned = [jnp.moveaxis(a, dim, 0) for a, dim in zip(arrays, dims)]
     both = jnp.concatenate([t.reshape(len(t), -1) for t in turned], axis=1)
-    out, at, finished = (lax.all_gather(both, axis, axis=0, tiled=True), 0, [])
+    out, at, finished = (
+        jnp.concatenate(
+            lax.all_to_all(jnp.stack([both] * lax.axis_size(axis)), axis, 0, 0), axis=0
+        ),
+        0,
+        [],
+    )
     for t, dim in zip(turned, dims):
         slab = out[:, at : at + t[0].size].reshape(-1, *t.shape[1:])
         finished.append(jnp.moveaxis(slab, 0, dim))

time: 251 us -> 367 us (1.46)
  waiting for transfers between devices: 71.7 us -> 166 us
  local copies, waits for them, and re-layouts: 22.1 us -> 42 us
    all_to_all x0 -> x1, waiting for transfers between devices: none -> 159 us  [turned_gather(): lax.all_to_all(jnp.stack([both] * lax.axis_size(axis)), axis, 0, 0)]
    all_gather x1 -> x0, waiting for transfers between devices: 71 us -> none  [turned_gather(): out, at, finished = (lax.all_gather(both, axis, axis=0, tiled=True), 0, [])]
    all_to_all x0 -> x1, starting transfers between devices: none -> 15.9 us  [turned_gather(): lax.all_to_all(jnp.stack([both] * lax.axis_size(axis)), axis, 0, 0)]
    split x1 -> x3, local copies, waits for them, and re-layouts: 6.02 us -> 18.9 us  [side_by_side(): jnp.split(lax.all_gather(both, axis, axis=dim, tiled=True), ends, axis=al...]
    all_to_all x1, starting transfers between devices: 27.8 us -> 18.5 us  [per_device(): lax.all_to_all(both, 'tp', split_axis=0, concat_axis=0, tiled=True)]
    all_to_all x1, waiting for transfers between devices: 0.01 us -> 6.28 us  [copy_for_each(): return lax.all_to_all(copies, axis, split_axis=0, concat_axis=0, tiled=True)]
    all_to_all x0 -> x1, local copies, waits for them, and re-layouts: none -> 6.05 us  [turned_gather(): lax.all_to_all(jnp.stack([both] * lax.axis_size(axis)), axis, 0, 0)]
    all_to_all x1, starting transfers between devices: 10.4 us -> 5.69 us  [copy_for_each(): return lax.all_to_all(copies, axis, split_axis=0, concat_axis=0, tiled=True)]
  transfers between devices with their start and end apart: 5 -> 5, of which waited for: 2 -> 3; matrix products, arithmetic and copies ran while one was open for 24% -> 21% of each run, Pallas kernels for 0% -> 0%
where the time goes in v1:
time: 367 us; the launch traced here: 366 us
  waiting for transfers between devices  166 us (45%)
  blocking collectives  49.7 us (14%)
  starting transfers between devices  44.3 us (12%)
  local copies, waits for them, and re-layouts  42 us (11%)
  matrix products  24.8 us (7%)
  other arithmetic  24.6 us (7%)
  between operations  14.5 us (4%)
    all_to_all x1, waiting for transfers between devices, turned_gather(): lax.all_to_all(jnp.stack([both] * lax.axis_size(axis)), axis, 0, 0)  159 us
    all_gather x2, blocking collectives, entering(): lax.all_gather(a.astype(kind), axis)  49.7 us
    another operation x1, other arithmetic, block_terms(): lax.linalg.triangular_solve(identity + corr_lower, jnp.broadcast_to(ident...  19.7 us
    split x3, local copies, waits for them, and re-layouts, side_by_side(): jnp.split(lax.all_gather(both, axis, axis=dim, tiled=True), ends, axis=al...  18.9 us
    all_to_all x1, starting transfers between devices, per_device(): lax.all_to_all(both, 'tp', split_axis=0, concat_axis=0, tiled=True)  18.5 us
    all_to_all x1, starting transfers between devices, turned_gather(): lax.all_to_all(jnp.stack([both] * lax.axis_size(axis)), axis, 0, 0)  15.9 us
    dot_general x5, matrix products, project(): jnp.dot(norm_result, weight, preferred_element_type=jnp.float32)  7.35 us
  transfers between devices with their start and end apart: 5, of which 3 were waited for; matrix products, arithmetic and copies ran while one was open for 21% of the time, Pallas kernels for 0%

profile of v1, /device:TPU:1, one launch (start us, length us, event | category | flops | bytes accessed | tf_op | source)
XLA Modules:
  0.0 365.7 jit_solution(1280896706267465372)
XLA Ops:
  6.5 0.9 copy.101
  7.4 0.9 copy.102
  8.3 0.9 copy.103
  9.2 0.9 copy.104
  10.0 0.9 copy.105
  11.0 0.8 bitcast_dynamic-update-slice_fusion.1
  11.8 0.8 bitcast_dynamic-update-slice_fusion
  12.5 2.5 stack.2
  15.1 15.9 %all-to-all-start.1 = ((bf16[16,128,896]{1,2,0:T(8,128)(2,1)}), bf16[16,128,896]{1,2,0:T(8,128)(2,1)}, u32[]{:S(2)}, u32[]{:S(2)}) async-start(bf16[16,128,896]{1,2,0:T(8,128)(2,1)} %stack.2), calls=%async_computation.1 | async-start | bytes 7340032 | tf_op jit(solution)/shard_map/all_to_all | solution.py:17
  31.8 158.6 %all-to-all-done.1 = bf16[16,128,896]{1,2,0:T(8,128)(2,1)} async-done(((bf16[16,128,896]{1,2,0:T(8,128)(2,1)}), bf16[16,128,896]{1,2,0:T(8,128)(2,1)}, u32[]{:S(2)}, u32[]{:S(2)}) %all-to-all-start.1) | async-done | bytes 3670048 | tf_op jit(solution)/shard_map/all_to_all | solution.py:17
  190.4 1.1 broadcast_in_dim.91
  191.5 5.7 %all-to-all-start = ((bf16[8,32,2048]{2,1,0:T(8,128)(2,1)}), bf16[8,32,2048]{2,1,0:T(8,128)(2,1)S(1)}, u32[]{:S(2)}, u32[]{:S(2)}) async-start(bf16[8,32,2048]{2,1,0:T(8,128)(2,1)} %broadcast_in_dim.91), calls=%async_computation | async-start | bytes 2097152 | tf_op jit(solution)/shard_map/all_to_all | solution.py:31
  197.2 6.0 %copy.106 = bf16[16,128,896]{2,1,0:T(8,128)(2,1)} copy(bf16[16,128,896]{1,2,0:T(8,128)(2,1)} %all-to-all-done.1) | data formatting | bytes 7340032 | tf_op jit(solution)/shard_map/all_to_all | solution.py:17
  203.3 1.3 slice_bitcast_fusion.1
  204.6 1.1 pad_maximum_fusion
  205.9 6.3 %all-to-all-done = bf16[8,32,2048]{2,1,0:T(8,128)(2,1)S(1)} async-done(((bf16[8,32,2048]{2,1,0:T(8,128)(2,1)}), bf16[8,32,2048]{2,1,0:T(8,128)(2,1)S(1)}, u32[]{:S(2)}, u32[]{:S(2)}) %all-to-all-start) | async-done | bytes 1048608 | tf_op jit(solution)/shard_map/all_to_all | solution.py:31
  212.2 0.3 multiply_reduce_fusion
  212.6 0.3 fusion.59
  212.9 0.4 fusion.100
  213.9 1.5 fusion.131
  215.4 1.5 convolution_convert_fusion.1
  216.8 1.5 convolution_convert_fusion.2
  218.3 1.5 convolution_convert_fusion.3
  219.8 4.2 %collective-permute-start = (bf16[15,512]{1,0:T(8,128)(2,1)S(1)}, bf16[15,512]{1,0:T(8,128)(2,1)S(1)}, u32[]{:S(2)}, u32[]{:S(2)}) collective-permute-start(bf16[15,512]{1,0:T(8,128)(2,1)S(1)} %fusion.115), channel_id=1, source_target_pairs={{0,32},{32,64},{64,96},{96,128},{128,160},{160,192},{192,224},{224... | collective-permute-start | bytes 46088 | tf_op jit(solution)/shard_map/ppermute | solution.py:48
  224.2 0.7 collective-permute-done
  225.3 0.2 divide_multiply_fusion
  226.1 19.7 %custom-call.3 = f32[1,4,1,64,64]{3,4,2,1,0:T(8,128)S(1)} custom-call(f32[1,4,1,64,64]{4,3,2,1,0:T(8,128)S(1)} %fusion.65), custom_call_target="InvertDiagBlocksLowerTriangular" | custom-call | tf_op jit(solution)/shard_map/triangular_solve | solution.py:110
  245.7 0.4 fusion.91
  246.3 0.3 convolution_bitcast_fusion.4
  246.7 9.7 %while.39 = (s32[]{:T(128)}, f32[1,128,128]{2,1,0:T(8,128)S(1)}, f32[1,128,128]{2,1,0:T(8,128)S(1)}, f32[4,1]{0,1:T(1,128)S(1)}, bf16[4,1,64,128]{3,2,1,0:T(8,12...) while((s32[]{:T(128)}, f32[1,128,128]{2,1,0:T(8,128)S(1)}, ...), condition=%wide.region_6.7_spmd.clone, body=%wide.region_5.6_spmd.clone.sunk | while | flops 8503299 | bytes 757378 | solution.py:263
  246.8 0.6 fusion.206
  247.4 0.9 fusion.208
  248.3 0.9 fusion.207
  249.2 0.6 fusion.206
  249.8 0.9 fusion.208
  250.7 0.9 fusion.207
  251.6 0.6 fusion.206
  252.2 0.9 fusion.208
  253.1 0.9 fusion.207
  254.0 0.6 fusion.206
  254.7 0.9 fusion.208
  255.6 0.9 fusion.207
  256.8 26.6 %all-gather = bf16[16,128,128]{2,1,0:T(8,128)(2,1)S(1)} all-gather(bf16[1,128,128]{2,1,0:T(8,128)(2,1)S(1)} %convert_element_type.116), channel_id=2, replica_groups=mesh['sp'=16,'fs'=4,'tp'=8] {'sp'}, dimensions={0}, use_global_device_ids=true | all-gather | bytes 557056 | tf_op jit(solution)/shard_map/all_gather | solution.py:54
  283.4 23.1 %all-gather.1 = bf16[16,128,128]{2,1,0:T(8,128)(2,1)S(1)} all-gather(bf16[1,128,128]{2,1,0:T(8,128)(2,1)S(1)} %convert_element_type.117), channel_id=3, replica_groups=mesh['sp'=16,'fs'=4,'tp'=8] {'sp'}, dimensions={0}, use_global_device_ids=true | all-gather | bytes 557056 | tf_op jit(solution)/shard_map/all_gather | solution.py:54
  306.4 7.4 %while.38 = (s32[]{:T(128)}, f32[1,128,128]{2,1,0:T(8,128)S(1)}, f32[4,1,64,128]{3,2,1,0:T(8,128)S(1)}, f32[4,1]{0,1:T(1,128)S(1)}, bf16[4,1,64,128]{3,2,1,0:T(8...) while((s32[]{:T(128)}, f32[1,128,128]{2,1,0:T(8,128)S(1)}, ...), condition=%wide.region_11.12_spmd, body=%wide.region_10.11_spmd.sunk | while | flops 7397378 | bytes 510085 | solution.py:266
  306.4 0.6 fusion.195
  307.3 0.8 fusion.196
  308.3 0.6 fusion.195
  309.2 0.8 fusion.196
  310.1 0.6 fusion.195
  311.0 0.8 fusion.196
  312.0 0.6 fusion.195
  312.8 0.8 fusion.196
  314.0 0.3 fusion.110
  314.3 1.5 fusion.90
  315.8 0.7 pad_maximum_fusion.1
  316.5 18.5 %all-to-all-start.2 = ((bf16[8,32,256]{2,1,0:T(8,128)(2,1)}), bf16[8,32,256]{2,1,0:T(8,128)(2,1)S(1)}, u32[]{:S(2)}, u32[]{:S(2)}) async-start(bf16[8,32,256]{2,1,0:T(8,128)(2,1)} %pad_maximum_fusion.1), calls=%async_computation.2 | async-start | bytes 262144 | tf_op jit(solution)/shard_map/all_to_all | solution.py:278
  334.9 5.9 %fusion.129 = (bf16[1024,2048]{0,1:T(8,128)(2,1)}, bf16[1024,2048]{0,1:T(8,128)(2,1)}) fusion(bf16[1024,4096]{0,1:T(8,128)(2,1)} %all-gather.4.cloned.1.call-done), kind=kLoop, calls=%fused_computation.205 | loop fusion | bytes 16777216 | tf_op jit(solution)/shard_map/split | solution.py:77
  340.9 6.5 %copy.123 = bf16[1024,2048]{1,0:T(8,128)(2,1)} copy(bf16[1024,2048]{0,1:T(8,128)(2,1)} %get-tuple-element.315) | data formatting | bytes 8388608 | tf_op jit(solution)/shard_map/split | solution.py:77
  347.3 6.5 %copy.122 = bf16[1024,2048]{1,0:T(8,128)(2,1)} copy(bf16[1024,2048]{0,1:T(8,128)(2,1)} %get-tuple-element.316) | data formatting | bytes 8388608 | tf_op jit(solution)/shard_map/split | solution.py:77
  353.9 3.0 fusion.98
  356.9 0.4 copy-done.1
  357.3 0.7 fusion.57
  358.0 0.8 reduce_sum.52
  (98 shorter events, 4.4 us)
Async XLA Ops:
  6.5 307.5 %copy-start = (bf16[1,128,128]{2,1,0:T(8,128)(2,1)S(1)}, bf16[1,128,128]{2,1,0:T(8,128)(2,1)}, u32[]{:S(2)}) copy-start(bf16[1,128,128]{2,1,0:T(8,128)(2,1)} %param.35) | copy-start | bytes 98308
  15.1 16.6 %copy-start.6 = (bf16[2048]{0:T(1024)(128)(2,1)S(1)}, bf16[2048]{0:T(1024)(128)(2,1)}, u32[]{:S(2)}) copy-start(bf16[2048]{0:T(1024)(128)(2,1)} %param.24) | copy-start | bytes 12292
  15.1 175.3 %copy-start.2 = (bf16[32,2048]{1,0:T(8,128)(2,1)S(1)}, bf16[32,2048]{1,0:T(8,128)(2,1)}, u32[]{:S(2)}) copy-start(bf16[32,2048]{1,0:T(8,128)(2,1)} %param.23) | copy-start | bytes 393220
  15.1 175.3 %all-to-all-start.1 = ((bf16[16,128,896]{1,2,0:T(8,128)(2,1)}), bf16[16,128,896]{1,2,0:T(8,128)(2,1)}, u32[]{:S(2)}, u32[]{:S(2)}) async-start(bf16[16,128,896]{1,2,0:T(8,128)(2,1)} %stack.2), calls=%async_computation.1 | async-start | bytes 7340032 | tf_op jit(solution)/shard_map/all_to_all | solution.py:17
  191.5 20.7 %all-to-all-start = ((bf16[8,32,2048]{2,1,0:T(8,128)(2,1)}), bf16[8,32,2048]{2,1,0:T(8,128)(2,1)S(1)}, u32[]{:S(2)}, u32[]{:S(2)}) async-start(bf16[8,32,2048]{2,1,0:T(8,128)(2,1)} %broadcast_in_dim.91), calls=%async_computation | async-start | bytes 2097152 | tf_op jit(solution)/shard_map/all_to_all | solution.py:31
  197.2 137.7 %all-gather.4.cloned.1.call-start = ((), (), s32[]{:S(2)}) async-start(), calls=%async_computation.3 | async-start | bytes 9437184 | tf_op jit(solution)/shard_map/all_gather | solution.py:77
  203.3 2.5 copy-start.5
  204.6 8.3 %copy-start.3 = (bf16[2048,8]{0,1:T(8,128)(2,1)S(1)}, bf16[2048,8]{0,1:T(8,128)(2,1)}, u32[]{:S(2)}) copy-start(bf16[2048,8]{0,1:T(8,128)(2,1)} %param.31) | copy-start | bytes 98308
  204.6 8.3 %copy-start.4 = (bf16[2048,8]{0,1:T(8,128)(2,1)S(1)}, bf16[2048,8]{0,1:T(8,128)(2,1)}, u32[]{:S(2)}) copy-start(bf16[2048,8]{0,1:T(8,128)(2,1)} %param.30) | copy-start | bytes 98308
  204.6 8.7 %copy-start.7 = (f32[256,1]{0,1:T(1,128)S(1)}, f32[256,1]{0,1:T(1,128)}, u32[]{:S(2)}) copy-start(f32[256,1]{0,1:T(1,128)} %param.34) | copy-start | bytes 3076
  219.8 5.1 %collective-permute-start = (bf16[15,512]{1,0:T(8,128)(2,1)S(1)}, bf16[15,512]{1,0:T(8,128)(2,1)S(1)}, u32[]{:S(2)}, u32[]{:S(2)}) collective-permute-start(bf16[15,512]{1,0:T(8,128)(2,1)S(1)} %fusion.115), channel_id=1, source_target_pairs={{0,32},{32,64},{64,96},{96,128},{128,160},{160,192},{192,224},{224... | collective-permute-start | bytes 46088 | tf_op jit(solution)/shard_map/ppermute | solution.py:48
  283.4 30.9 %copy-start.8 = (f32[128]{0:T(128)S(1)}, f32[128]{0:T(128)}, u32[]{:S(2)}) copy-start(f32[128]{0:T(128)} %param.36) | copy-start | bytes 1540
  283.4 30.9 %copy-start.9 = (f32[128]{0:T(128)S(1)}, f32[128]{0:T(128)}, u32[]{:S(2)}) copy-start(f32[128]{0:T(128)} %param.37) | copy-start | bytes 1540
  316.5 37.4 %all-to-all-start.2 = ((bf16[8,32,256]{2,1,0:T(8,128)(2,1)}), bf16[8,32,256]{2,1,0:T(8,128)(2,1)S(1)}, u32[]{:S(2)}, u32[]{:S(2)}) async-start(bf16[8,32,256]{2,1,0:T(8,128)(2,1)} %pad_maximum_fusion.1), calls=%async_computation.2 | async-start | bytes 262144 | tf_op jit(solution)/shard_map/all_to_all | solution.py:278
  353.9 3.5 copy-start.1
Sparse Core Ops, SparseCore 0:
  205.8 61.5 all-gather.3
